TPU v7x, 32 devices: a whole 2x2x4 slice. The times are simulated.
32 devices in a mesh: sp: 8 (over z, y), tp: 4 (over x, core).
Axes of the slice: x: 2, y: 2, z: 4, core: 2. Of those that a mesh axis runs over, the one named last changes fastest.
Arguments:
- stream: bfloat16 [3072, 2048], P(('sp', 'tp')), may hold values from -6 to 6
- query_projected: bfloat16 [3072, 1024], P('sp', 'tp'), may hold values from -6 to 6
- key_projected: bfloat16 [3072, 1024], P('sp', 'tp'), may hold values from -6 to 6
- value_projected: bfloat16 [3072, 1024], P('sp', 'tp'), may hold values from -6 to 6
- gate_projected: bfloat16 [3072, 1024], P('sp', 'tp'), may hold values from -6 to 6
- strength_logits: bfloat16 [8, 3072], P('tp', 'sp'), may hold values from -7 to 4
- decay_preactivation: bfloat16 [8, 3072], P('tp', 'sp'), may hold values from -9 to 9
- extra_log_decay: float32 [8, 3072], P('tp', 'sp'), may hold values from -0.7 to 0
- head_decay_rate: float32 [8], P('tp'), may hold values from 0 to 0.1
- head_norm_gain: float32 [128], replicated, may hold values from 0.1 to 1.9
- head_output_matrix: bfloat16 [1024, 2048], P('tp'), may hold values from -0.1875 to 0.1875
- feed_norm_gain: float32 [2048], replicated, may hold values from 0.1 to 1.9
- gate_matrix: bfloat16 [2048, 5632], P('sp', 'tp'), may hold values from -0.125 to 0.125
- up_matrix: bfloat16 [2048, 5632], P('sp', 'tp'), may hold values from -0.125 to 0.125
- down_matrix: bfloat16 [5632, 2048], P('tp', 'sp'), may hold values from -0.078125 to 0.078125
Outputs:
- result: bfloat16 [3072, 2048], P(('sp', 'tp'))
All inputs are finite; a program needn't handle non-finite values.
Results may differ from a plain program's by a relative error of at most 0.015.
Values may be sent and summed in bfloat16 or wider, within the bound.
No kernel may reach another device: no remote copies, remote signals or barrier semaphores. Data moves between devices by JAX's collectives and lax.ppermute only.
A program may use at most 128 MiB of HBM per device.

v0:
```python
import jax
import jax.numpy as jnp
from jax import lax
from jax.sharding import PartitionSpec as P

HEAD = 128
BLOCK = 64
PRECISION_FULL = lax.Precision.HIGHEST
EPSILON = 1e-06


def from_behind(value, axis, by):
    size = lax.axis_size(axis)
    pairs = [(i, i + by) for i in range(size) if 0 <= i + by < size]
    return lax.ppermute(value, axis, pairs)


def unit_rows(tensor):
    return tensor * lax.rsqrt(jnp.sum(tensor * tensor, axis=-1, keepdims=True) + EPSILON)


def rms_scale(tensor):
    return tensor * lax.rsqrt(jnp.mean(tensor * tensor, axis=-1, keepdims=True) + EPSILON)


def unit_lower_inverse(strict_lower):
    size = strict_lower.shape[-1]
    row = jnp.arange(size)[:, None]
    column = jnp.arange(size)[None, :]

    def corner(half):
        same_pair = row // (2 * half) == column // (2 * half)
        return jnp.where(same_pair & (row // half != column // half), strict_lower, 0.0)

    inverse = jnp.eye(size, dtype=jnp.float32) - corner(1)
    half = 2
    while half < size:
        left = jnp.einsum("hnij,hnjk->hnik", inverse, corner(half), precision=PRECISION_FULL)
        inverse = inverse - jnp.einsum("hnij,hnjk->hnik", left, inverse, precision=PRECISION_FULL)
        half *= 2
    return inverse


def swap(value, axis, bit):
    size = lax.axis_size(axis)
    return lax.ppermute(value, axis, [(i, i ^ bit) for i in range(size)])


def relative_order(count):
    order = [0]
    bit = count // 2
    while bit:
        order = order + [place ^ bit for place in order]
        bit //= 2
    return order


def gather_relative(own):
    bit = lax.axis_size("tp") // 2
    while bit:
        own = jnp.concatenate([own, swap(own, "tp", bit)], axis=0)
        bit //= 2
    return own


def scatter_relative(left_rows, matrix):
    size = lax.axis_size("tp")
    if size == 1:
        return jnp.dot(left_rows, matrix, preferred_element_type=jnp.float32)
    half = left_rows.shape[0] // 2
    leaving = jnp.dot(left_rows[half:], matrix, preferred_element_type=jnp.float32)
    arrived = swap(leaving.astype(jnp.bfloat16), "tp", 1)
    total = jnp.dot(left_rows[:half], matrix, preferred_element_type=jnp.float32)
    total = total + arrived.astype(jnp.float32)
    bit = 2
    while bit < size:
        half = total.shape[0] // 2
        arrived = swap(total[half:].astype(jnp.bfloat16), "tp", bit)
        total = total[:half] + arrived.astype(jnp.float32)
        bit *= 2
    return total


def inflow_of_earlier(matrix_product, running_state):
    size = lax.axis_size("sp")
    width = running_state.shape[-1]
    pair = jnp.concatenate([matrix_product, running_state], axis=-1)
    pair = from_behind(pair.astype(jnp.bfloat16), "sp", 1).astype(jnp.float32)
    by = 1
    while by < size - 1:
        matrix, state = (pair[..., :width], pair[..., width:])
        last = 2 * by >= size - 1
        sent = (state if last else pair).astype(jnp.bfloat16)
        earlier = from_behind(sent, "sp", by).astype(jnp.float32)
        moved = jnp.einsum("hij,hjk->hik", matrix, earlier, precision=PRECISION_FULL)
        if last:
            pair = jnp.concatenate([matrix, state + moved], axis=-1)
        else:
            pair = jnp.concatenate([moved[..., :width], state + moved[..., width:]], axis=-1)
        by *= 2
    return pair[..., width:]


def block_correction(
    unit_queries,
    unit_keys,
    complete_values,
    strength_logits,
    decay_preactivation,
    extra_log_decay,
    head_decay_rate,
):
    head_count, length, head_width = unit_queries.shape
    block_count = length // BLOCK

    def to_blocks(tensor):
        return tensor.reshape((head_count, block_count, BLOCK) + tensor.shape[2:])

    beta_gate = jax.nn.sigmoid(strength_logits.astype(jnp.float32))
    decay_logarithm = (
        -head_decay_rate[:, None] * jax.nn.softplus(decay_preactivation.astype(jnp.float32))
        + extra_log_decay
    )
    query_block = to_blocks(unit_queries)
    key_block = to_blocks(unit_keys)
    value_block = to_blocks(complete_values)
    beta_block = to_blocks(beta_gate)
    cumulative = jnp.cumsum(to_blocks(decay_logarithm), axis=-1)
    causal = jnp.tril(jnp.ones((BLOCK, BLOCK), bool))
    strict = jnp.tril(jnp.ones((BLOCK, BLOCK), bool), -1)
    spread = cumulative[..., :, None] - cumulative[..., None, :]
    damping = jnp.where(causal, jnp.exp(jnp.where(causal, spread, 0.0)), 0.0)
    key_beta = key_block * beta_block[..., None]
    lower_part = jnp.einsum(
        "hnid,hnjd->hnij", key_beta, key_block, precision=PRECISION_FULL
    ) * jnp.where(strict, damping, 0.0)
    right_side = jnp.concatenate(
        [value_block * beta_block[..., None], key_beta * jnp.exp(cumulative)[..., None]], axis=-1
    )
    solved = jnp.einsum(
        "hnij,hnjd->hnid", unit_lower_inverse(lower_part), right_side, precision=PRECISION_FULL
    )
    target_values = solved[..., :head_width]
    householder_weights = solved[..., head_width:]
    inner_scores = (
        jnp.einsum("hnid,hnjd->hnij", query_block, key_block, precision=PRECISION_FULL) * damping
    )
    decayed_queries = query_block * jnp.exp(cumulative)[..., None]
    closing_log_decay = cumulative[..., -1:]
    decayed_keys = key_block * jnp.exp(closing_log_decay - cumulative)[..., None]
    return (
        decayed_queries,
        decayed_keys,
        target_values,
        householder_weights,
        inner_scores,
        closing_log_decay,
    )


def local_recurrence(
    query_projected,
    key_projected,
    value_projected,
    strength_logits,
    decay_preactivation,
    extra_log_decay,
    head_decay_rate,
):
    head_count = strength_logits.shape[0]
    tok_count = strength_logits.shape[1]

    def split_heads(tensor):
        return tensor.reshape(tok_count, head_count, HEAD).transpose(1, 0, 2).astype(jnp.float32)

    unit_queries = unit_rows(split_heads(query_projected)) * HEAD ** (-0.5)
    unit_keys = unit_rows(split_heads(key_projected))
    complete_values = split_heads(value_projected)
    score_terms = block_correction(
        unit_queries,
        unit_keys,
        complete_values,
        strength_logits,
        decay_preactivation,
        extra_log_decay,
        head_decay_rate,
    )
    identity = jnp.broadcast_to(jnp.eye(HEAD, dtype=jnp.float32), (head_count, HEAD, HEAD))

    def advance(carry, items):
        running_state, matrix_product = carry
        (
            decayed_queries,
            decayed_keys,
            target_values,
            householder_weights,
            inner_scores,
            closing_log_decay,
        ) = items
        new_state = target_values - jnp.einsum(
            "fdc,fcj->fdj", householder_weights, running_state, precision=PRECISION_FULL
        )
        layer_output = jnp.einsum(
            "fdc,fcj->fdj", decayed_queries, running_state, precision=PRECISION_FULL
        )
        layer_output = layer_output + jnp.einsum(
            "hij,hjv->hiv", inner_scores, new_state, precision=PRECISION_FULL
        )
        passed_state = decayed_queries - jnp.einsum(
            "hij,hjk->hik", inner_scores, householder_weights, precision=PRECISION_FULL
        )
        decay_span = jnp.einsum(
            "fdc,fcj->fdj", passed_state, matrix_product, precision=PRECISION_FULL
        )
        decay_factor = jnp.exp(closing_log_decay)[:, :, None]
        step_map = decay_factor * identity - jnp.einsum(
            "hik,hij->hkj", decayed_keys, householder_weights, precision=PRECISION_FULL
        )
        running_state = decay_factor * running_state + jnp.einsum(
            "xwp,xws->xps", decayed_keys, new_state, precision=PRECISION_FULL
        )
        matrix_product = jnp.einsum(
            "hij,hjk->hik", step_map, matrix_product, precision=PRECISION_FULL
        )
        return ((running_state, matrix_product), (layer_output, decay_span))

    moved = tuple((jnp.moveaxis(tensor, 1, 0) for tensor in score_terms))
    zeros_state = jnp.zeros((head_count, HEAD, HEAD), jnp.float32)
    (running_state, matrix_product), (block_outputs, decay_spans) = lax.scan(
        advance, (zeros_state, identity), moved
    )

    def merge_blocks(tensor):
        return jnp.moveaxis(tensor, 0, 1).reshape(head_count, tok_count, HEAD)

    return (
        merge_blocks(block_outputs),
        merge_blocks(decay_spans),
        matrix_product,
        running_state,
        identity,
    )


def body(
    stream,
    query_projected,
    key_projected,
    value_projected,
    gate_projected,
    strength_logits,
    decay_preactivation,
    extra_log_decay,
    head_decay_rate,
    head_norm_gain,
    head_output_matrix,
    feed_norm_gain,
    gate_matrix,
    up_matrix,
    down_matrix,
):
    gate_whole = lax.all_gather(gate_matrix, "sp", axis=0, tiled=True)
    up_whole = lax.all_gather(up_matrix, "sp", axis=0, tiled=True)
    down_whole = lax.all_gather(down_matrix, "sp", axis=1, tiled=True)
    block_outputs, decay_spans, matrix_product, running_state, _ = local_recurrence(
        query_projected,
        key_projected,
        value_projected,
        strength_logits,
        decay_preactivation,
        extra_log_decay,
        head_decay_rate,
    )
    state_inflow = inflow_of_earlier(matrix_product, running_state)
    attention_output = block_outputs + jnp.einsum(
        "qwc,qcn->qwn", decay_spans, state_inflow, precision=PRECISION_FULL
    )
    head_count = attention_output.shape[0]
    tok_count = attention_output.shape[1]
    normed_heads = rms_scale(attention_output) * head_norm_gain
    gated = normed_heads.transpose(1, 0, 2).reshape(tok_count, head_count * HEAD)
    mixed = (gated * jax.nn.silu(gate_projected.astype(jnp.float32))).astype(jnp.bfloat16)
    tp_size = lax.axis_size("tp")
    tp_index = lax.axis_index("tp")
    chunks = mixed.reshape(tp_size, tok_count // tp_size, head_count * HEAD)
    ordered = jnp.concatenate(
        [
            lax.dynamic_index_in_dim(chunks, tp_index ^ place, 0, keepdims=False)
            for place in relative_order(tp_size)
        ],
        axis=0,
    )
    branch = scatter_relative(ordered, head_output_matrix)
    residual_own = stream.astype(jnp.float32) + branch
    normed_own = (rms_scale(residual_own) * feed_norm_gain).astype(jnp.bfloat16)
    whole_rows = gather_relative(normed_own)
    gate_total = jnp.dot(whole_rows, gate_whole, preferred_element_type=jnp.float32)
    up_total = jnp.dot(whole_rows, up_whole, preferred_element_type=jnp.float32)
    hidden = (jax.nn.silu(gate_total) * up_total).astype(jnp.bfloat16)
    ffn_own = scatter_relative(hidden, down_whole)
    return (residual_own + ffn_own).astype(jnp.bfloat16)


def solution(mesh):
    placed = (
        P(("sp", "tp"), None),
        P("sp", "tp"),
        P("sp", "tp"),
        P("sp", "tp"),
        P("sp", "tp"),
        P("tp", "sp"),
        P("tp", "sp"),
        P("tp", "sp"),
        P("tp"),
        P(),
        P("tp", None),
        P(),
        P("sp", "tp"),
        P("sp", "tp"),
        P("tp", "sp"),
    )
    return jax.shard_map(
        body, mesh=mesh, in_specs=placed, out_specs=P(("sp", "tp"), None), check_vma=False
    )
```

profile of v0, /device:TPU:0, one launch (start us, length us, event | category | flops | bytes accessed | tf_op | source)
XLA Modules:
  0.0 326.3 jit_solution(2462705551969413879)
XLA Ops:
  20.0 26.2 %while.17 = (s32[]{:T(128)}, f32[2,128,128]{2,1,0:T(8,128)S(1)}, f32[2,128,128]{2,1,0:T(8,128)S(1)}, f32[6,2,64,128]{3,2,0,1:T(8,128)}, f32[6,2,64,128]{3,2,0,1:...) while((s32[]{:T(128)}, f32[2,128,128]{2,1,0:T(8,128)S(1)}, ...), condition=%wide.region_4.5_spmd.clone, body=%wide.region_3.4_spmd.clone.sunk | while | flops 201605120 | bytes 2758829 | solution.py:229
  20.0 1.1 convolution_subtract_fusion.11
  24.4 1.1 convolution_subtract_fusion.11
  27.2 0.9 fusion.206
  28.7 1.1 convolution_subtract_fusion.11
  31.6 0.9 fusion.206
  33.1 1.1 convolution_subtract_fusion.11
  37.5 1.1 convolution_subtract_fusion.11
  41.8 1.1 convolution_subtract_fusion.11
  44.7 0.9 fusion.206
  46.3 5.0 %collective-permute-start = (bf16[2,128,256]{2,1,0:T(8,128)(2,1)S(1)}, bf16[2,128,256]{2,1,0:T(8,128)(2,1)S(1)}, u32[]{:S(2)}, u32[]{:S(2)}) collective-permute-start(bf16[2,128,256]{2,1,0:T(8,128)(2,1)S(1)} %pad_maximum_fusion.6), channel_id=1, source_target_pairs={{0,4},{4,8},{8,12},{12,16},{16,20},{20,24},{24,28},{1,5},{5,9},{9,... | collective-permute-start | bytes 393224 | tf_op jit(solution)/shard_map/ppermute | solution.py:15
  51.3 5.5 %collective-permute-done = bf16[2,128,256]{2,1,0:T(8,128)(2,1)S(1)} collective-permute-done((bf16[2,128,256]{2,1,0:T(8,128)(2,1)S(1)}, bf16[2,128,256]{2,1,0:T(8,128)(2,1)S(1)}, u32[]{:S(2)}, u32[]{:S(2)}) %collective-permute-start) | collective-permute-done | bytes 131104 | tf_op jit(solution)/shard_map/ppermute | solution.py:15
  56.9 4.4 %collective-permute-start.1 = (bf16[2,128,256]{2,1,0:T(8,128)(2,1)S(1)}, bf16[2,128,256]{2,1,0:T(8,128)(2,1)S(1)}, u32[]{:S(2)}, u32[]{:S(2)}) collective-permute-start(bf16[2,128,256]{2,1,0:T(8,128)(2,1)S(1)} %collective-permute-done), channel_id=1, source_target_pairs={{0,4},{4,8},{8,12},{12,16},{16,20},{20,24},{24,28},{1,5},{5,9},{9,... | collective-permute-start | bytes 393224 | tf_op jit(solution)/shard_map/ppermute | solution.py:15
  61.2 5.4 %collective-permute-done.1 = bf16[2,128,256]{2,1,0:T(8,128)(2,1)S(1)} collective-permute-done((bf16[2,128,256]{2,1,0:T(8,128)(2,1)S(1)}, bf16[2,128,256]{2,1,0:T(8,128)(2,1)S(1)}, u32[]{:S(2)}, u32[]{:S(2)}) %collective-permute-start.1) | collective-permute-done | bytes 131104 | tf_op jit(solution)/shard_map/ppermute | solution.py:15
  66.9 6.0 %collective-permute-start.2 = (bf16[2,128,256]{2,1,0:T(8,128)(2,1)S(1)}, bf16[2,128,256]{2,1,0:T(8,128)(2,1)S(1)}, u32[]{:S(2)}, u32[]{:S(2)}) collective-permute-start(bf16[2,128,256]{2,1,0:T(8,128)(2,1)S(1)} %pad_maximum_fusion.7), channel_id=1, source_target_pairs={{0,8},{4,12},{8,16},{12,20},{16,24},{20,28},{1,9},{5,13},{9,17},{1... | collective-permute-start | bytes 393224 | tf_op jit(solution)/shard_map/ppermute | solution.py:15
  72.9 5.4 %collective-permute-done.2 = bf16[2,128,256]{2,1,0:T(8,128)(2,1)S(1)} collective-permute-done((bf16[2,128,256]{2,1,0:T(8,128)(2,1)S(1)}, bf16[2,128,256]{2,1,0:T(8,128)(2,1)S(1)}, u32[]{:S(2)}, u32[]{:S(2)}) %collective-permute-start.2) | collective-permute-done | bytes 131104 | tf_op jit(solution)/shard_map/ppermute | solution.py:15
  78.6 20.5 %collective-permute-start.3 = (bf16[2,128,128]{2,1,0:T(8,128)(2,1)S(1)}, bf16[2,128,128]{2,1,0:T(8,128)(2,1)S(1)}, u32[]{:S(2)}, u32[]{:S(2)}) collective-permute-start(bf16[2,128,128]{2,1,0:T(8,128)(2,1)S(1)} %fusion.128), channel_id=1, source_target_pairs={{0,16},{4,20},{8,24},{12,28},{1,17},{5,21},{9,25},{13,29},{2,18},{... | collective-permute-start | bytes 196616 | tf_op jit(solution)/shard_map/ppermute | solution.py:15
  99.3 2.9 collective-permute-done.3
  104.1 2.3 collective-permute-done.4
  106.9 11.1 %collective-permute-done.5 = bf16[96,2048]{1,0:T(8,128)(2,1)S(1)} collective-permute-done((bf16[96,2048]{1,0:T(8,128)(2,1)S(1)}, bf16[96,2048]{1,0:T(8,128)(2,1)S(1)}, u32[]{:S(2)}, u32[]{:S(2)}) %collective-permute-start.5) | collective-permute-done | bytes 393248 | tf_op jit(solution)/shard_map/ppermute | solution.py:46
  118.8 10.0 %collective-permute-done.6 = bf16[96,2048]{1,0:T(8,128)(2,1)S(1)} collective-permute-done((bf16[96,2048]{1,0:T(8,128)(2,1)S(1)}, bf16[96,2048]{1,0:T(8,128)(2,1)S(1)}, u32[]{:S(2)}, u32[]{:S(2)}) %collective-permute-start.6) | collective-permute-done | bytes 393248 | tf_op jit(solution)/shard_map/ppermute | solution.py:46
  129.6 1.8 collective-permute-done.7
  131.4 7.1 %fusion.47 = f32[384,1408]{1,0:T(8,128)} fusion(bf16[2048,1408]{1,0:T(8,128)(2,1)} %all-gather.4.cloned.1.call-done, bf16[192,2048]{1,0:T(8,128)(2,1)} %collective-permute-done.7, bf16[96,2048]{1,0:T(8,128)(2,1)} %copy-done.7, bf16[96,2048]{1,0:T(8,128)(2,1)} %copy-done.2), kind=kOutput, calls=%fused_computation.75 | convolution fusion | flops 2219311104 | bytes 9502720 | tf_op jit(solution)/shard_map/dot_general | solution.py:297
  138.5 67.4 %all-gather.6.cloned.1.call-done = bf16[2048,1408]{1,0:T(8,128)(2,1)} async-done(((bf16[256,1408]{1,0:T(8,128)(2,1)}), bf16[2048,1408]{1,0:T(8,128)(2,1)}) %all-gather.6.cloned.1.call-update) | async-done | bytes 5767184 | tf_op jit(solution)/shard_map/all_gather | solution.py:263
  206.0 7.4 %multiply_convert_fusion = bf16[384,1408]{1,0:T(8,128)(2,1)} fusion(f32[384,1408]{1,0:T(8,128)} %fusion.47, bf16[2048,1408]{1,0:T(8,128)(2,1)} %all-gather.6.cloned.1.call-done, bf16[192,2048]{1,0:T(8,128)(2,1)} %collective-permute-done.7, bf16[96,2048]{1,0:T(8,128)(2,1)} %copy-done.7, bf16[96,2048]{1,0:T(8,128)(2,1)} %copy-done.2), kind=kOutput, calls=%fused_computation.46 | convolution fusion | flops 2222555136 | bytes 10584064 | tf_op jit(solution)/shard_map/dot_general | solution.py:298
  213.4 86.0 %all-gather.8.cloned.1.call-done = bf16[1408,2048]{1,0:T(8,128)(2,1)} async-done(((bf16[1408,256]{1,0:T(8,128)(2,1)}), bf16[1408,2048]{1,0:T(8,128)(2,1)}) %all-gather.8.cloned.1.call-update) | async-done | bytes 5767184 | tf_op jit(solution)/shard_map/all_gather | solution.py:264
  299.4 4.3 %convolution_convert_fusion = bf16[192,2048]{1,0:T(8,128)(2,1)S(1)} fusion(bf16[1408,2048]{1,0:T(8,128)(2,1)} %all-gather.8.cloned.1.call-done, bf16[384,1408]{1,0:T(8,128)(2,1)} %multiply_convert_fusion), kind=kOutput, calls=%fused_computation.44 | convolution fusion | flops 1107689472 | bytes 7094272 | tf_op jit(solution)/shard_map/dot_general | solution.py:71
  303.8 2.3 collective-permute-done.8
  306.1 1.4 convert_add_fusion
  307.5 1.6 collective-permute-start.9
  309.1 9.6 %collective-permute-done.9 = bf16[96,2048]{1,0:T(8,128)(2,1)S(1)} collective-permute-done((bf16[96,2048]{1,0:T(8,128)(2,1)S(1)}, bf16[96,2048]{1,0:T(8,128)(2,1)S(1)}, u32[]{:S(2)}, u32[]{:S(2)}) %collective-permute-start.9) | collective-permute-done | bytes 393248 | tf_op jit(solution)/shard_map/ppermute | solution.py:46
  318.7 1.0 fusion.40
  (167 shorter events, 34.4 us)
Async XLA Ops:
  6.5 97.1 %copy-start = (bf16[256,2048]{1,0:T(8,128)(2,1)S(1)}, bf16[256,2048]{1,0:T(8,128)(2,1)}, u32[]{:S(2)}) copy-start(bf16[256,2048]{1,0:T(8,128)(2,1)} %param.27) | copy-start | bytes 3145732
  6.5 2.3 copy-start.16
  6.5 2.4 copy-start.12
  6.5 2.4 copy-start.11
  6.5 2.5 copy-start.3
  6.5 3.0 copy-start.13
  6.6 124.9 %all-gather.4.cloned.1.call-start = ((), (), s32[]{:S(2)}) async-start(), calls=%async_computation | async-start | bytes 6488064 | tf_op jit(solution)/shard_map/all_gather | solution.py:262
  7.3 198.7 %all-gather.6.cloned.1.call-start = ((), (), s32[]{:S(2)}) async-start(), calls=%async_computation.1 | async-start | bytes 6488064 | tf_op jit(solution)/shard_map/all_gather | solution.py:263
  8.0 291.3 %all-gather.8.cloned.1.call-start = ((), (), s32[]{:S(2)}) async-start(), calls=%async_computation.2 | async-start | bytes 6488064 | tf_op jit(solution)/shard_map/all_gather | solution.py:264
  14.4 2.3 copy-start.4
  14.9 2.1 copy-start.8
  46.2 52.9 %copy-start.5 = (f32[6,2,64,128]{3,2,0,1:T(8,128)S(1)}, f32[6,2,64,128]{3,2,0,1:T(8,128)}, u32[]{:S(2)}) copy-start(f32[6,2,64,128]{3,2,0,1:T(8,128)} %get-tuple-element.70) | copy-start | bytes 1179652
  46.2 56.2 %copy-start.6 = (f32[6,2,64,128]{3,2,0,1:T(8,128)S(1)}, f32[6,2,64,128]{3,2,0,1:T(8,128)}, u32[]{:S(2)}) copy-start(f32[6,2,64,128]{3,2,0,1:T(8,128)} %get-tuple-element.71) | copy-start | bytes 1179652
  46.3 10.6 %collective-permute-start = (bf16[2,128,256]{2,1,0:T(8,128)(2,1)S(1)}, bf16[2,128,256]{2,1,0:T(8,128)(2,1)S(1)}, u32[]{:S(2)}, u32[]{:S(2)}) collective-permute-start(bf16[2,128,256]{2,1,0:T(8,128)(2,1)S(1)} %pad_maximum_fusion.6), channel_id=1, source_target_pairs={{0,4},{4,8},{8,12},{12,16},{16,20},{20,24},{24,28},{1,5},{5,9},{9,... | collective-permute-start | bytes 393224 | tf_op jit(solution)/shard_map/ppermute | solution.py:15
  56.9 9.8 %collective-permute-start.1 = (bf16[2,128,256]{2,1,0:T(8,128)(2,1)S(1)}, bf16[2,128,256]{2,1,0:T(8,128)(2,1)S(1)}, u32[]{:S(2)}, u32[]{:S(2)}) collective-permute-start(bf16[2,128,256]{2,1,0:T(8,128)(2,1)S(1)} %collective-permute-done), channel_id=1, source_target_pairs={{0,4},{4,8},{8,12},{12,16},{16,20},{20,24},{24,28},{1,5},{5,9},{9,... | collective-permute-start | bytes 393224 | tf_op jit(solution)/shard_map/ppermute | solution.py:15
  66.8 36.3 %copy-start.14 = (f32[128]{0:T(128)S(1)}, f32[128]{0:T(128)}, u32[]{:S(2)}) copy-start(f32[128]{0:T(128)} %param.26) | copy-start | bytes 1540
  66.9 11.4 %collective-permute-start.2 = (bf16[2,128,256]{2,1,0:T(8,128)(2,1)S(1)}, bf16[2,128,256]{2,1,0:T(8,128)(2,1)S(1)}, u32[]{:S(2)}, u32[]{:S(2)}) collective-permute-start(bf16[2,128,256]{2,1,0:T(8,128)(2,1)S(1)} %pad_maximum_fusion.7), channel_id=1, source_target_pairs={{0,8},{4,12},{8,16},{12,20},{16,24},{20,28},{1,9},{5,13},{9,17},{1... | collective-permute-start | bytes 393224 | tf_op jit(solution)/shard_map/ppermute | solution.py:15
  78.6 24.8 %copy-start.9 = (bf16[384,256]{1,0:T(8,128)(2,1)S(1)}, bf16[384,256]{1,0:T(8,128)(2,1)}, u32[]{:S(2)}) copy-start(bf16[384,256]{1,0:T(8,128)(2,1)} %param.21) | copy-start | bytes 589828
  78.6 23.6 %collective-permute-start.3 = (bf16[2,128,128]{2,1,0:T(8,128)(2,1)S(1)}, bf16[2,128,128]{2,1,0:T(8,128)(2,1)S(1)}, u32[]{:S(2)}, u32[]{:S(2)}) collective-permute-start(bf16[2,128,128]{2,1,0:T(8,128)(2,1)S(1)} %fusion.128), channel_id=1, source_target_pairs={{0,16},{4,20},{8,24},{12,28},{1,17},{5,21},{9,25},{13,29},{2,18},{... | collective-permute-start | bytes 196616 | tf_op jit(solution)/shard_map/ppermute | solution.py:15
  104.0 14.0 %copy-start.1 = (bf16[96,2048]{1,0:T(8,128)(2,1)S(1)}, bf16[96,2048]{1,0:T(8,128)(2,1)}, u32[]{:S(2)}) copy-start(bf16[96,2048]{1,0:T(8,128)(2,1)} %param.17) | copy-start | bytes 1179652
  104.0 2.4 collective-permute-start.4
  106.3 11.9 %copy-start.10 = (f32[2048]{0:T(1024)S(1)}, f32[2048]{0:T(1024)}, u32[]{:S(2)}) copy-start(f32[2048]{0:T(1024)} %param.28) | copy-start | bytes 24580
  106.8 11.2 %collective-permute-start.5 = (bf16[96,2048]{1,0:T(8,128)(2,1)S(1)}, bf16[96,2048]{1,0:T(8,128)(2,1)S(1)}, u32[]{:S(2)}, u32[]{:S(2)}) collective-permute-start(bf16[96,2048]{1,0:T(8,128)(2,1)S(1)} %slice.148), channel_id=1, source_target_pairs={{0,2},{1,3},{2,0},{3,1},{4,6},{5,7},{6,4},{7,5},{8,10},{9,11},{10,... | collective-permute-start | bytes 1179656 | tf_op jit(solution)/shard_map/ppermute | solution.py:46
  118.5 10.4 %copy-start.2 = (bf16[96,2048]{1,0:T(8,128)(2,1)}, bf16[96,2048]{1,0:T(8,128)(2,1)S(1)}, u32[]{:S(2)}) copy-start(bf16[96,2048]{1,0:T(8,128)(2,1)S(1)} %multiply_convert_fusion.1) | copy-start | bytes 1179652
  118.5 10.4 %collective-permute-start.6 = (bf16[96,2048]{1,0:T(8,128)(2,1)S(1)}, bf16[96,2048]{1,0:T(8,128)(2,1)S(1)}, u32[]{:S(2)}, u32[]{:S(2)}) collective-permute-start(bf16[96,2048]{1,0:T(8,128)(2,1)S(1)} %multiply_convert_fusion.1), channel_id=1, source_target_pairs={{0,2},{1,3},{2,0},{3,1},{4,6},{5,7},{6,4},{7,5},{8,10},{9,11},{10,... | collective-permute-start | bytes 1179656 | tf_op jit(solution)/shard_map/ppermute | solution.py:46
  128.9 0.7 copy-start.7
  128.9 2.5 collective-permute-start.7
  299.4 6.7 %copy-start.15 = (bf16[1408,2048]{1,0:T(8,128)(2,1)S(1)}, bf16[1408,2048]{1,0:T(8,128)(2,1)}, u32[]{:S(2)}) copy-start(bf16[1408,2048]{1,0:T(8,128)(2,1)} %all-gather.8.cloned.1.call-done) | copy-start | bytes 17301508
  299.4 6.7 %copy-start.17 = (bf16[384,1408]{1,0:T(8,128)(2,1)S(1)}, bf16[384,1408]{1,0:T(8,128)(2,1)}, u32[]{:S(2)}) copy-start(bf16[384,1408]{1,0:T(8,128)(2,1)} %multiply_convert_fusion) | copy-start | bytes 3244036
  303.7 2.4 collective-permute-start.8
  307.5 11.2 %collective-permute-start.9 = (bf16[96,2048]{1,0:T(8,128)(2,1)S(1)}, bf16[96,2048]{1,0:T(8,128)(2,1)S(1)}, u32[]{:S(2)}, u32[]{:S(2)}) collective-permute-start(bf16[96,2048]{1,0:T(8,128)(2,1)S(1)} %slice.147), channel_id=1, source_target_pairs={{0,2},{1,3},{2,0},{3,1},{4,6},{5,7},{6,4},{7,5},{8,10},{9,11},{10,... | collective-permute-start | bytes 1179656 | tf_op jit(solution)/shard_map/ppermute | solution.py:46
Sparse Core Ops, SparseCore 0:
  9.5 99.7 all-gather.3
  111.5 94.4 all-gather.5
  208.0 91.2 all-gather.7
where the time goes:
time: 327 us; the launch traced here: 326 us
  waiting for transfers between devices  212 us (65%)
  matrix products  55.6 us (17%)
  starting transfers between devices  38.3 us (12%)
  between operations  13.8 us (4%)
  other arithmetic  3.82 us (1%)
    all_gather x1, waiting for transfers between devices, body(): down_whole = lax.all_gather(down_matrix, 'sp', axis=1, tiled=True)  86 us
    all_gather x1, waiting for transfers between devices, body(): up_whole = lax.all_gather(up_matrix, 'sp', axis=0, tiled=True)  67.4 us
    ppermute x6, waiting for transfers between devices, swap(): return lax.ppermute(value, axis, [(i, i ^ bit) for i in range(size)])  37.2 us
    ppermute x4, starting transfers between devices, from_behind(): return lax.ppermute(value, axis, pairs)  35.9 us
    ppermute x4, waiting for transfers between devices, from_behind(): return lax.ppermute(value, axis, pairs)  19.2 us
    dot_general x1, matrix products, body(): up_total = jnp.dot(whole_rows, up_whole, preferred_element_type=jnp.float32)  7.38 us
    dot_general x1, matrix products, body(): jnp.dot(whole_rows, gate_whole, preferred_element_type=jnp.float32)  7.12 us
  transfers between devices with their start and end apart: 13, of which 12 were waited for; matrix products, arithmetic and copies ran while one was open for 17% of the time, Pallas kernels for 0%

commit v1 on v0

--- a/solution.py
+++ b/solution.py
@@ -260,7 +260,9 @@
     down_matrix,
 ):
     gate_whole = lax.all_gather(gate_matrix, "sp", axis=0, tiled=True)
-    up_whole = lax.all_gather(up_matrix, "sp", axis=0, tiled=True)
+    up_whole = jnp.concatenate(
+        lax.all_to_all(jnp.stack([up_matrix] * lax.axis_size("sp")), "sp", 0, 0), axis=0
+    )
     down_whole = lax.all_gather(down_matrix, "sp", axis=1, tiled=True)
     block_outputs, decay_spans, matrix_product, running_state, _ = local_recurrence(
         query_projected,

time: 327 us -> 337 us (1.031)
  starting transfers between devices: 38.3 us -> 190 us
  waiting for transfers between devices: 212 us -> 66.3 us
  local copies, waits for them, and re-layouts: 2.49 us -> 6.51 us
    ppermute x4, starting transfers between devices: 35.9 us -> 178 us  [from_behind(): return lax.ppermute(value, axis, pairs)]
    all_gather x1, waiting for transfers between devices: 86 us -> 10.8 us  [body(): down_whole = lax.all_gather(down_matrix, 'sp', axis=1, tiled=True)]
    all_gather x1 -> x0, waiting for transfers between devices: 67.4 us -> none  [body(): up_whole = lax.all_gather(up_matrix, 'sp', axis=0, tiled=True)]
    all_to_all x0 -> x1, starting transfers between devices: none -> 7.45 us  [body(): lax.all_to_all(jnp.stack([up_matrix] * lax.axis_size('sp')), 'sp', 0, 0)]
    another operation x0 -> x1, local copies, waits for them, and re-layouts: none -> 4 us  [body(): jnp.stack([up_matrix] * lax.axis_size('sp'))]
  transfers between devices with their start and end apart: 13 -> 13, of which waited for: 12 -> 11; matrix products, arithmetic and copies ran while one was open for 17% -> 17% of each run, Pallas kernels for 0% -> 0%
where the time goes in v1:
time: 337 us
  starting transfers between devices  190 us (56%)
  waiting for transfers between devices  66.3 us (20%)
  matrix products  55.8 us (17%)
  between operations  14.1 us (4%)
  local copies, waits for them, and re-layouts  6.51 us (2%)
  other arithmetic  3.82 us (1%)
    ppermute x4, starting transfers between devices, from_behind(): return lax.ppermute(value, axis, pairs)  178 us
    ppermute x6, waiting for transfers between devices, swap(): return lax.ppermute(value, axis, [(i, i ^ bit) for i in range(size)])  34.8 us
    ppermute x4, waiting for transfers between devices, from_behind(): return lax.ppermute(value, axis, pairs)  19.4 us
    all_gather x1, waiting for transfers between devices, body(): down_whole = lax.all_gather(down_matrix, 'sp', axis=1, tiled=True)  10.8 us
    dot_general x1, matrix products, body(): up_total = jnp.dot(whole_rows, up_whole, preferred_element_type=jnp.float32)  7.53 us
    all_to_all x1, starting transfers between devices, body(): lax.all_to_all(jnp.stack([up_matrix] * lax.axis_size('sp')), 'sp', 0, 0)  7.45 us
    dot_general x1, matrix products, body(): jnp.dot(whole_rows, gate_whole, preferred_element_type=jnp.float32)  7.14 us
  transfers between devices with their start and end apart: 13, of which 11 were waited for; matrix products, arithmetic and copies ran while one was open for 17% of the time, Pallas kernels for 0%

profile of v1, /device:TPU:0, one launch (start us, length us, event | category | flops | bytes accessed | tf_op | source)
XLA Modules:
  0.0 336.7 jit_solution(8140016382743054053)
XLA Ops:
  7.3 4.0 %stack.2 = bf16[8,256,1408]{2,1,0:T(8,128)(2,1)} broadcast(bf16[256,1408]{1,0:T(8,128)(2,1)} %param.30), dimensions={1,2} | broadcast | bytes 6488064 | tf_op jit(solution)/shard_map/stack | solution.py:264
  11.3 7.5 %all-to-all-start = ((bf16[8,256,1408]{2,1,0:T(8,128)(2,1)}), bf16[8,256,1408]{2,1,0:T(8,128)(2,1)}, u32[]{:S(2)}, u32[]{:S(2)}) async-start(bf16[8,256,1408]{2,1,0:T(8,128)(2,1)} %stack.2), calls=%async_computation | async-start | bytes 11534336 | tf_op jit(solution)/shard_map/all_to_all | solution.py:264
  30.7 26.2 %while.17 = (s32[]{:T(128)}, f32[2,128,128]{2,1,0:T(8,128)S(1)}, f32[2,128,128]{2,1,0:T(8,128)S(1)}, f32[6,2,64,128]{3,2,0,1:T(8,128)}, f32[6,2,64,128]{3,2,0,1:...) while((s32[]{:T(128)}, f32[2,128,128]{2,1,0:T(8,128)S(1)}, ...), condition=%wide.region_4.5_spmd.clone, body=%wide.region_3.4_spmd.clone.sunk | while | flops 201605120 | bytes 2758829 | solution.py:229
  30.7 1.1 convolution_subtract_fusion.11
  35.1 1.1 convolution_subtract_fusion.11
  39.5 1.1 convolution_subtract_fusion.11
  43.9 1.1 convolution_subtract_fusion.11
  48.2 1.1 convolution_subtract_fusion.11
  52.6 1.1 convolution_subtract_fusion.11
  57.1 4.1 %collective-permute-start = (bf16[2,128,256]{2,1,0:T(8,128)(2,1)S(1)}, bf16[2,128,256]{2,1,0:T(8,128)(2,1)S(1)}, u32[]{:S(2)}, u32[]{:S(2)}) collective-permute-start(bf16[2,128,256]{2,1,0:T(8,128)(2,1)S(1)} %pad_maximum_fusion.6), channel_id=1, source_target_pairs={{0,4},{4,8},{8,12},{12,16},{16,20},{20,24},{24,28},{1,5},{5,9},{9,... | collective-permute-start | bytes 393224 | tf_op jit(solution)/shard_map/ppermute | solution.py:15
  61.1 9.6 %collective-permute-done = bf16[2,128,256]{2,1,0:T(8,128)(2,1)S(1)} collective-permute-done((bf16[2,128,256]{2,1,0:T(8,128)(2,1)S(1)}, bf16[2,128,256]{2,1,0:T(8,128)(2,1)S(1)}, u32[]{:S(2)}, u32[]{:S(2)}) %collective-permute-start) | collective-permute-done | bytes 131104 | tf_op jit(solution)/shard_map/ppermute | solution.py:15
  70.7 92.2 %collective-permute-start.1 = (bf16[2,128,256]{2,1,0:T(8,128)(2,1)S(1)}, bf16[2,128,256]{2,1,0:T(8,128)(2,1)S(1)}, u32[]{:S(2)}, u32[]{:S(2)}) collective-permute-start(bf16[2,128,256]{2,1,0:T(8,128)(2,1)S(1)} %collective-permute-done), channel_id=1, source_target_pairs={{0,4},{4,8},{8,12},{12,16},{16,20},{20,24},{24,28},{1,5},{5,9},{9,... | collective-permute-start | bytes 393224 | tf_op jit(solution)/shard_map/ppermute | solution.py:15
  162.8 3.1 collective-permute-done.1
  166.2 62.4 %collective-permute-start.2 = (bf16[2,128,256]{2,1,0:T(8,128)(2,1)S(1)}, bf16[2,128,256]{2,1,0:T(8,128)(2,1)S(1)}, u32[]{:S(2)}, u32[]{:S(2)}) collective-permute-start(bf16[2,128,256]{2,1,0:T(8,128)(2,1)S(1)} %pad_maximum_fusion.7), channel_id=1, source_target_pairs={{0,8},{4,12},{8,16},{12,20},{16,24},{20,28},{1,9},{5,13},{9,17},{1... | collective-permute-start | bytes 393224 | tf_op jit(solution)/shard_map/ppermute | solution.py:15
  228.6 5.0 %collective-permute-done.2 = bf16[2,128,256]{2,1,0:T(8,128)(2,1)S(1)} collective-permute-done((bf16[2,128,256]{2,1,0:T(8,128)(2,1)S(1)}, bf16[2,128,256]{2,1,0:T(8,128)(2,1)S(1)}, u32[]{:S(2)}, u32[]{:S(2)}) %collective-permute-start.2) | collective-permute-done | bytes 131104 | tf_op jit(solution)/shard_map/ppermute | solution.py:15
  233.9 19.0 %collective-permute-start.3 = (bf16[2,128,128]{2,1,0:T(8,128)(2,1)S(1)}, bf16[2,128,128]{2,1,0:T(8,128)(2,1)S(1)}, u32[]{:S(2)}, u32[]{:S(2)}) collective-permute-start(bf16[2,128,128]{2,1,0:T(8,128)(2,1)S(1)} %fusion.128), channel_id=1, source_target_pairs={{0,16},{4,20},{8,24},{12,28},{1,17},{5,21},{9,25},{13,29},{2,18},{... | collective-permute-start | bytes 196616 | tf_op jit(solution)/shard_map/ppermute | solution.py:15
  253.1 1.7 collective-permute-done.3
  256.6 2.3 collective-permute-done.4
  259.3 1.4 collective-permute-start.5
  260.8 9.8 %collective-permute-done.5 = bf16[96,2048]{1,0:T(8,128)(2,1)S(1)} collective-permute-done((bf16[96,2048]{1,0:T(8,128)(2,1)S(1)}, bf16[96,2048]{1,0:T(8,128)(2,1)S(1)}, u32[]{:S(2)}, u32[]{:S(2)}) %collective-permute-start.5) | collective-permute-done | bytes 393248 | tf_op jit(solution)/shard_map/ppermute | solution.py:46
  271.0 1.4 collective-permute-start.6
  272.5 9.0 %collective-permute-done.6 = bf16[96,2048]{1,0:T(8,128)(2,1)S(1)} collective-permute-done((bf16[96,2048]{1,0:T(8,128)(2,1)S(1)}, bf16[96,2048]{1,0:T(8,128)(2,1)S(1)}, u32[]{:S(2)}, u32[]{:S(2)}) %collective-permute-start.6) | collective-permute-done | bytes 393248 | tf_op jit(solution)/shard_map/ppermute | solution.py:46
  282.2 1.8 collective-permute-done.7
  284.1 7.1 %fusion.47 = f32[384,1408]{1,0:T(8,128)} fusion(bf16[2048,1408]{1,0:T(8,128)(2,1)} %all-gather.3.cloned.1.call-done, bf16[192,2048]{1,0:T(8,128)(2,1)} %collective-permute-done.7, bf16[96,2048]{1,0:T(8,128)(2,1)} %copy-done.7, bf16[96,2048]{1,0:T(8,128)(2,1)} %copy-done.2), kind=kOutput, calls=%fused_computation.75 | convolution fusion | flops 2219311104 | bytes 9502720 | tf_op jit(solution)/shard_map/dot_general | solution.py:299
  291.2 7.5 %multiply_convert_fusion = bf16[384,1408]{1,0:T(8,128)(2,1)} fusion(f32[384,1408]{1,0:T(8,128)} %fusion.47, bf16[2048,1408]{1,0:T(8,128)(2,1)} %bitcast.24, bf16[192,2048]{1,0:T(8,128)(2,1)} %collective-permute-done.7, bf16[96,2048]{1,0:T(8,128)(2,1)} %copy-done.7, bf16[96,2048]{1,0:T(8,128)(2,1)} %copy-done.2), kind=kOutput, calls=%fused_computation.46 | convolution fusion | flops 2222555136 | bytes 10584064 | tf_op jit(solution)/shard_map/dot_general | solution.py:300
  298.7 10.8 %all-gather.5.cloned.1.call-done = bf16[1408,2048]{1,0:T(8,128)(2,1)} async-done(((bf16[1408,256]{1,0:T(8,128)(2,1)}), bf16[1408,2048]{1,0:T(8,128)(2,1)}) %all-gather.5.cloned.1.call-update) | async-done | bytes 5767184 | tf_op jit(solution)/shard_map/all_gather | solution.py:266
  309.5 4.3 %convolution_convert_fusion = bf16[192,2048]{1,0:T(8,128)(2,1)S(1)} fusion(bf16[1408,2048]{1,0:T(8,128)(2,1)} %all-gather.5.cloned.1.call-done, bf16[384,1408]{1,0:T(8,128)(2,1)} %multiply_convert_fusion), kind=kOutput, calls=%fused_computation.44 | convolution fusion | flops 1107689472 | bytes 7094272 | tf_op jit(solution)/shard_map/dot_general | solution.py:71
  313.9 2.3 collective-permute-done.8
  316.2 1.4 convert_add_fusion
  317.6 1.6 collective-permute-start.9
  319.2 9.6 %collective-permute-done.9 = bf16[96,2048]{1,0:T(8,128)(2,1)S(1)} collective-permute-done((bf16[96,2048]{1,0:T(8,128)(2,1)S(1)}, bf16[96,2048]{1,0:T(8,128)(2,1)S(1)}, u32[]{:S(2)}, u32[]{:S(2)}) %collective-permute-start.9) | collective-permute-done | bytes 393248 | tf_op jit(solution)/shard_map/ppermute | solution.py:46
  328.9 1.0 fusion.40
  (167 shorter events, 35.9 us)
Async XLA Ops:
  6.5 249.6 %copy-start = (bf16[256,2048]{1,0:T(8,128)(2,1)S(1)}, bf16[256,2048]{1,0:T(8,128)(2,1)}, u32[]{:S(2)}) copy-start(bf16[256,2048]{1,0:T(8,128)(2,1)} %param.27) | copy-start | bytes 3145732
  6.5 277.5 %all-gather.3.cloned.1.call-start = ((), (), s32[]{:S(2)}) async-start(), calls=%async_computation.1 | async-start | bytes 6488064 | tf_op jit(solution)/shard_map/all_gather | solution.py:262
  11.3 8.3 %copy-start.16 = (f32[2]{0:T(128)S(1)}, f32[2]{0:T(128)}, u32[]{:S(2)}) copy-start(f32[2]{0:T(128)} %param.25) | copy-start | bytes 28
  11.3 8.3 %copy-start.11 = (f32[2,384]{1,0:T(2,128)S(1)}, f32[2,384]{1,0:T(2,128)}, u32[]{:S(2)}) copy-start(f32[2,384]{1,0:T(2,128)} %param.24) | copy-start | bytes 9220
  11.3 8.4 %copy-start.12 = (bf16[2,384]{1,0:T(2,128)(2,1)S(1)}, bf16[2,384]{1,0:T(2,128)(2,1)}, u32[]{:S(2)}) copy-start(bf16[2,384]{1,0:T(2,128)(2,1)} %param.23) | copy-start | bytes 4612
  11.3 8.5 %copy-start.3 = (bf16[384,256]{1,0:T(8,128)(2,1)S(1)}, bf16[384,256]{1,0:T(8,128)(2,1)}, u32[]{:S(2)}) copy-start(bf16[384,256]{1,0:T(8,128)(2,1)} %param.19) | copy-start | bytes 589828
  11.3 9.0 %copy-start.13 = (bf16[2,384]{1,0:T(2,128)(2,1)S(1)}, bf16[2,384]{1,0:T(2,128)(2,1)}, u32[]{:S(2)}) copy-start(bf16[2,384]{1,0:T(2,128)(2,1)} %param.22) | copy-start | bytes 4612
  11.3 279.9 %all-to-all-start = ((bf16[8,256,1408]{2,1,0:T(8,128)(2,1)}), bf16[8,256,1408]{2,1,0:T(8,128)(2,1)}, u32[]{:S(2)}, u32[]{:S(2)}) async-start(bf16[8,256,1408]{2,1,0:T(8,128)(2,1)} %stack.2), calls=%async_computation | async-start | bytes 11534336 | tf_op jit(solution)/shard_map/all_to_all | solution.py:264
  18.7 290.8 %all-gather.5.cloned.1.call-start = ((), (), s32[]{:S(2)}) async-start(), calls=%async_computation.2 | async-start | bytes 6488064 | tf_op jit(solution)/shard_map/all_gather | solution.py:266
  25.1 2.2 copy-start.4
  25.6 2.1 copy-start.8
  57.0 195.9 %copy-start.5 = (f32[6,2,64,128]{3,2,0,1:T(8,128)S(1)}, f32[6,2,64,128]{3,2,0,1:T(8,128)}, u32[]{:S(2)}) copy-start(f32[6,2,64,128]{3,2,0,1:T(8,128)} %get-tuple-element.70) | copy-start | bytes 1179652
  57.0 198.0 %copy-start.6 = (f32[6,2,64,128]{3,2,0,1:T(8,128)S(1)}, f32[6,2,64,128]{3,2,0,1:T(8,128)}, u32[]{:S(2)}) copy-start(f32[6,2,64,128]{3,2,0,1:T(8,128)} %get-tuple-element.71) | copy-start | bytes 1179652
  57.1 13.6 %collective-permute-start = (bf16[2,128,256]{2,1,0:T(8,128)(2,1)S(1)}, bf16[2,128,256]{2,1,0:T(8,128)(2,1)S(1)}, u32[]{:S(2)}, u32[]{:S(2)}) collective-permute-start(bf16[2,128,256]{2,1,0:T(8,128)(2,1)S(1)} %pad_maximum_fusion.6), channel_id=1, source_target_pairs={{0,4},{4,8},{8,12},{12,16},{16,20},{20,24},{24,28},{1,5},{5,9},{9,... | collective-permute-start | bytes 393224 | tf_op jit(solution)/shard_map/ppermute | solution.py:15
  70.7 95.3 %collective-permute-start.1 = (bf16[2,128,256]{2,1,0:T(8,128)(2,1)S(1)}, bf16[2,128,256]{2,1,0:T(8,128)(2,1)S(1)}, u32[]{:S(2)}, u32[]{:S(2)}) collective-permute-start(bf16[2,128,256]{2,1,0:T(8,128)(2,1)S(1)} %collective-permute-done), channel_id=1, source_target_pairs={{0,4},{4,8},{8,12},{12,16},{16,20},{20,24},{24,28},{1,5},{5,9},{9,... | collective-permute-start | bytes 393224 | tf_op jit(solution)/shard_map/ppermute | solution.py:15
  166.1 89.5 %copy-start.14 = (f32[128]{0:T(128)S(1)}, f32[128]{0:T(128)}, u32[]{:S(2)}) copy-start(f32[128]{0:T(128)} %param.26) | copy-start | bytes 1540
  166.2 67.4 %collective-permute-start.2 = (bf16[2,128,256]{2,1,0:T(8,128)(2,1)S(1)}, bf16[2,128,256]{2,1,0:T(8,128)(2,1)S(1)}, u32[]{:S(2)}, u32[]{:S(2)}) collective-permute-start(bf16[2,128,256]{2,1,0:T(8,128)(2,1)S(1)} %pad_maximum_fusion.7), channel_id=1, source_target_pairs={{0,8},{4,12},{8,16},{12,20},{16,24},{20,28},{1,9},{5,13},{9,17},{1... | collective-permute-start | bytes 393224 | tf_op jit(solution)/shard_map/ppermute | solution.py:15
  233.9 22.1 %copy-start.9 = (bf16[384,256]{1,0:T(8,128)(2,1)S(1)}, bf16[384,256]{1,0:T(8,128)(2,1)}, u32[]{:S(2)}) copy-start(bf16[384,256]{1,0:T(8,128)(2,1)} %param.21) | copy-start | bytes 589828
  233.9 20.9 %collective-permute-start.3 = (bf16[2,128,128]{2,1,0:T(8,128)(2,1)S(1)}, bf16[2,128,128]{2,1,0:T(8,128)(2,1)S(1)}, u32[]{:S(2)}, u32[]{:S(2)}) collective-permute-start(bf16[2,128,128]{2,1,0:T(8,128)(2,1)S(1)} %fusion.128), channel_id=1, source_target_pairs={{0,16},{4,20},{8,24},{12,28},{1,17},{5,21},{9,25},{13,29},{2,18},{... | collective-permute-start | bytes 196616 | tf_op jit(solution)/shard_map/ppermute | solution.py:15
  256.5 14.0 %copy-start.1 = (bf16[96,2048]{1,0:T(8,128)(2,1)S(1)}, bf16[96,2048]{1,0:T(8,128)(2,1)}, u32[]{:S(2)}) copy-start(bf16[96,2048]{1,0:T(8,128)(2,1)} %param.17) | copy-start | bytes 1179652
  256.5 2.4 collective-permute-start.4
  258.9 11.9 %copy-start.10 = (f32[2048]{0:T(1024)S(1)}, f32[2048]{0:T(1024)}, u32[]{:S(2)}) copy-start(f32[2048]{0:T(1024)} %param.28) | copy-start | bytes 24580
  259.3 11.2 %collective-permute-start.5 = (bf16[96,2048]{1,0:T(8,128)(2,1)S(1)}, bf16[96,2048]{1,0:T(8,128)(2,1)S(1)}, u32[]{:S(2)}, u32[]{:S(2)}) collective-permute-start(bf16[96,2048]{1,0:T(8,128)(2,1)S(1)} %slice.148), channel_id=1, source_target_pairs={{0,2},{1,3},{2,0},{3,1},{4,6},{5,7},{6,4},{7,5},{8,10},{9,11},{10,... | collective-permute-start | bytes 1179656 | tf_op jit(solution)/shard_map/ppermute | solution.py:46
  271.0 10.5 %copy-start.2 = (bf16[96,2048]{1,0:T(8,128)(2,1)}, bf16[96,2048]{1,0:T(8,128)(2,1)S(1)}, u32[]{:S(2)}) copy-start(bf16[96,2048]{1,0:T(8,128)(2,1)S(1)} %multiply_convert_fusion.1) | copy-start | bytes 1179652
  271.0 10.5 %collective-permute-start.6 = (bf16[96,2048]{1,0:T(8,128)(2,1)S(1)}, bf16[96,2048]{1,0:T(8,128)(2,1)S(1)}, u32[]{:S(2)}, u32[]{:S(2)}) collective-permute-start(bf16[96,2048]{1,0:T(8,128)(2,1)S(1)} %multiply_convert_fusion.1), channel_id=1, source_target_pairs={{0,2},{1,3},{2,0},{3,1},{4,6},{5,7},{6,4},{7,5},{8,10},{9,11},{10,... | collective-permute-start | bytes 1179656 | tf_op jit(solution)/shard_map/ppermute | solution.py:46
  281.5 0.7 copy-start.7
  281.6 2.5 collective-permute-start.7
  309.5 6.7 %copy-start.15 = (bf16[1408,2048]{1,0:T(8,128)(2,1)S(1)}, bf16[1408,2048]{1,0:T(8,128)(2,1)}, u32[]{:S(2)}) copy-start(bf16[1408,2048]{1,0:T(8,128)(2,1)} %all-gather.5.cloned.1.call-done) | copy-start | bytes 17301508
  309.5 6.7 %copy-start.17 = (bf16[384,1408]{1,0:T(8,128)(2,1)S(1)}, bf16[384,1408]{1,0:T(8,128)(2,1)}, u32[]{:S(2)}) copy-start(bf16[384,1408]{1,0:T(8,128)(2,1)} %multiply_convert_fusion) | copy-start | bytes 3244036
  313.8 2.4 collective-permute-start.8
  317.6 11.2 %collective-permute-start.9 = (bf16[96,2048]{1,0:T(8,128)(2,1)S(1)}, bf16[96,2048]{1,0:T(8,128)(2,1)S(1)}, u32[]{:S(2)}, u32[]{:S(2)}) collective-permute-start(bf16[96,2048]{1,0:T(8,128)(2,1)S(1)} %slice.147), channel_id=1, source_target_pairs={{0,2},{1,3},{2,0},{3,1},{4,6},{5,7},{6,4},{7,5},{8,10},{9,11},{10,... | collective-permute-start | bytes 1179656 | tf_op jit(solution)/shard_map/ppermute | solution.py:46
Sparse Core Ops, SparseCore 0:
  9.5 199.5 all-gather.2
  211.1 98.3 all-gather.4
